TPU v7x, 128 devices: a whole 4x4x4 slice. The times are simulated.
128 devices in a mesh: tp: 16 (over z, x), dp: 8 (over y, core).
Axes of the slice: x: 4, y: 4, z: 4, core: 2. Of those that a mesh axis runs over, the one named last changes fastest.
Arguments:
- stream_in: bfloat16 [256, 4096], P('tp', 'dp'), may hold values from -21 to 21
- hidden_state: float32 [2, 256, 4096], P(None, 'dp', 'tp'), may hold values from -6 to 6
- convolution_window_state: bfloat16 [2, 256, 3, 4096], P(None, 'dp', None, 'tp'), may hold values from -6 to 6
- norm_gain: float32 [2, 4096], P(None, 'dp'), may hold values from 0.1 to 1.9
- path_weight: bfloat16 [2, 4096, 4096], P(None, 'dp', 'tp'), may hold values from -0.09375 to 0.09375
- output_gate_weight: bfloat16 [2, 4096, 4096], P(None, 'dp', 'tp'), may hold values from -0.09375 to 0.09375
- conv_taps: float32 [2, 4, 4096], P(None, None, 'tp'), may hold values from -3 to 3
- recur_map: float32 [2, 64, 64, 64], P(None, 'tp'), may hold values from -0.75 to 0.75
- input_map: float32 [2, 64, 64, 64], P(None, 'tp'), may hold values from -0.75 to 0.75
- decay_logit: float32 [2, 4096], P(None, 'tp'), may hold values from 1 to 6
- out_weight: bfloat16 [2, 4096, 4096], P(None, 'tp', 'dp'), may hold values from -0.09375 to 0.09375
Outputs:
- stream_out: bfloat16 [256, 4096], P('tp', 'dp')
- hidden_next: float32 [2, 256, 4096], P(None, 'dp', 'tp')
- conv_next: bfloat16 [2, 256, 3, 4096], P(None, 'dp', None, 'tp')
All inputs are finite; a program needn't handle non-finite values.
Results may differ from a plain program's by a relative error of at most 0.019.
Values may be sent and summed in bfloat16 or wider, within the bound.
No kernel may reach another device: no remote copies, remote signals or barrier semaphores. Data moves between devices by JAX's collectives and lax.ppermute only.
A program may use at most 64 MiB of HBM per device.

v0:
```python
import jax
import jax.numpy as jnp
from jax import lax
from jax.sharding import PartitionSpec as P

D = 4096
TAPS = 4


EPS = 1e-06


def from_everyone(array, axis):
    copies = jnp.broadcast_to(array, (lax.axis_size(axis), *array.shape))
    return lax.all_to_all(copies, axis, split_axis=0, concat_axis=0, tiled=True)


def of_everyone(array, axis):
    everything = from_everyone(array, axis)
    return jnp.sum(everything, axis=0)


def in_order(parts, dim):
    parts = jnp.moveaxis(parts, 0, dim)
    shape = parts.shape
    return parts.reshape(*shape[:dim], shape[dim] * shape[dim + 1], *shape[dim + 2 :])


def collect(array, axis, dim):
    return in_order(from_everyone(array, axis), dim)


def in_blocks(array, dim, devices):
    before, after = (array.shape[:dim], array.shape[dim + 1 :])
    return jnp.moveaxis(array.reshape(*before, devices, -1, *after), dim, 0)


def sum_at_owner(array, axis, dim):
    parts = in_blocks(array, dim, lax.axis_size(axis))
    arrived = lax.all_to_all(parts, axis, split_axis=0, concat_axis=0, tiled=True)
    return arrived.astype(jnp.float32).sum(axis=0)


def scaled(rows, gain):
    rowsf = rows.astype(jnp.float32)
    sumsq = of_everyone(jnp.sum(rowsf * rowsf, axis=1), "dp")
    return (rowsf * lax.rsqrt(sumsq / D + EPS)[:, None] * gain[None, :]).astype(jnp.bfloat16)


def shard_inputs(normed, path_w, gate_branch_matrix):
    return jnp.concatenate(
        [
            jnp.dot(normed, path_w, preferred_element_type=jnp.float32),
            jnp.dot(normed, gate_branch_matrix, preferred_element_type=jnp.float32),
        ],
        axis=1,
    )


def split_inputs(rows, gain, path_w, gate_branch_matrix):
    normed = scaled(rows, gain)
    return shard_inputs(collect(normed, "tp", 0), path_w, gate_branch_matrix)


def recur_tail(partial_value, hidden, buffer, taps, recur_w, input_matrix, logit, out_w):
    width = partial_value.shape[1] // 2
    summed = sum_at_owner(partial_value.astype(jnp.bfloat16), "dp", 0)
    zpath = summed[:, :width].astype(jnp.bfloat16)
    zgate = summed[:, width:].astype(jnp.bfloat16)
    batch = zpath.shape[0]
    conv = zpath.astype(jnp.float32) * taps[TAPS - 1][None, :]
    for j in range(TAPS - 1):
        conv = conv + buffer[:, j].astype(jnp.float32) * taps[j][None, :]
    new_buffer = jnp.concatenate([buffer[:, 1:], zpath[:, None, :]], axis=1)
    cblocks = conv.reshape(batch, recur_w.shape[0], recur_w.shape[1])
    rgate = jax.nn.sigmoid(
        jnp.einsum("bnc,ncd->bnd", cblocks, recur_w, precision=lax.Precision.HIGHEST).reshape(
            batch, width
        )
    )
    igate = jax.nn.sigmoid(
        jnp.einsum("bnc,ncd->bnd", cblocks, input_matrix, precision=lax.Precision.HIGHEST).reshape(
            batch, width
        )
    )
    loga = 8.0 * rgate * jax.nn.log_sigmoid(logit)[None, :]
    new_hidden = jnp.exp(loga) * hidden + jnp.sqrt(-jnp.expm1(2.0 * loga)) * (igate * conv)
    mixed = (new_hidden * jax.nn.gelu(zgate.astype(jnp.float32))).astype(jnp.bfloat16)
    update = jnp.dot(collect(mixed, "dp", 0), out_w, preferred_element_type=jnp.float32)
    return (update, new_hidden, new_buffer)


def per_device(
    stream_in,
    hidden_state,
    convolution_window_state,
    norm_gain,
    path_weight,
    output_gate_weight,
    conv_taps,
    recur_map,
    input_map,
    decay_logit,
    out_weight,
):
    stream = stream_in
    partial_value = split_inputs(stream, norm_gain[0], path_weight[0], output_gate_weight[0])
    update, hidden_first, buffer_first = recur_tail(
        partial_value,
        hidden_state[0],
        convolution_window_state[0],
        conv_taps[0],
        recur_map[0],
        input_map[0],
        decay_logit[0],
        out_weight[0],
    )
    stream = (
        stream.astype(jnp.float32) + sum_at_owner(update.astype(jnp.bfloat16), "tp", 0)
    ).astype(jnp.bfloat16)
    partial_value = split_inputs(stream, norm_gain[1], path_weight[1], output_gate_weight[1])
    update, hidden_second, buffer_second = recur_tail(
        partial_value,
        hidden_state[1],
        convolution_window_state[1],
        conv_taps[1],
        recur_map[1],
        input_map[1],
        decay_logit[1],
        out_weight[1],
    )
    stream = (
        stream.astype(jnp.float32) + sum_at_owner(update.astype(jnp.bfloat16), "tp", 0)
    ).astype(jnp.bfloat16)
    return (
        stream,
        jnp.stack([hidden_first, hidden_second]),
        jnp.stack([buffer_first, buffer_second]),
    )


def solution(mesh):
    placed = (
        P("tp", "dp"),
        P(None, "dp", "tp"),
        P(None, "dp", None, "tp"),
        P(None, "dp"),
        P(None, "dp", "tp"),
        P(None, "dp", "tp"),
        P(None, None, "tp"),
        P(None, "tp", None, None),
        P(None, "tp", None, None),
        P(None, "tp"),
        P(None, "tp", "dp"),
    )
    return jax.shard_map(
        per_device,
        mesh=mesh,
        in_specs=placed,
        out_specs=(P("tp", "dp"), P(None, "dp", "tp"), P(None, "dp", None, "tp")),
        check_vma=False,
    )
```

profile of v0, /device:TPU:0, one launch (start us, length us, event | category | flops | bytes accessed | tf_op | source)
XLA Modules:
  0.0 123.4 jit_solution(2130089506699500946)
XLA Ops:
  0.6 0.9 fusion.40
  2.1 4.6 %all-to-all-start = ((f32[8,1,16]{2,1,0:T(1,128)}), f32[8,1,16]{2,1,0:T(1,128)S(1)}, u32[]{:S(2)}, u32[]{:S(2)}) async-start(f32[8,1,16]{2,1,0:T(1,128)} %broadcast_in_dim.28), calls=%async_computation | async-start | bytes 8192 | tf_op jit(solution)/shard_map/all_to_all | solution.py:15
  6.7 0.8 fusion.78
  7.5 4.5 %all-to-all-done = f32[8,1,16]{2,1,0:T(1,128)S(1)} async-done(((f32[8,1,16]{2,1,0:T(1,128)}), f32[8,1,16]{2,1,0:T(1,128)S(1)}, u32[]{:S(2)}, u32[]{:S(2)}) %all-to-all-start) | async-done | bytes 544 | tf_op jit(solution)/shard_map/all_to_all | solution.py:15
  12.0 0.8 fusion.42
  12.8 0.7 broadcast_in_dim.29
  13.5 8.0 %all-to-all-start.1 = ((bf16[16,16,512]{2,1,0:T(8,128)(2,1)}), bf16[16,16,512]{2,1,0:T(8,128)(2,1)S(1)}, u32[]{:S(2)}, u32[]{:S(2)}) async-start(bf16[16,16,512]{2,1,0:T(8,128)(2,1)} %broadcast_in_dim.29), calls=%async_computation.1 | async-start | bytes 524288 | tf_op jit(solution)/shard_map/all_to_all | solution.py:15
  21.5 8.7 %all-to-all-done.1 = bf16[16,16,512]{2,1,0:T(8,128)(2,1)S(1)} async-done(((bf16[16,16,512]{2,1,0:T(8,128)(2,1)}), bf16[16,16,512]{2,1,0:T(8,128)(2,1)S(1)}, u32[]{:S(2)}, u32[]{:S(2)}) %all-to-all-start.1) | async-done | bytes 262176 | tf_op jit(solution)/shard_map/all_to_all | solution.py:15
  31.4 3.5 %all-to-all-start.2 = ((bf16[8,32,512]{2,1,0:T(8,128)(2,1)}), bf16[8,32,512]{2,1,0:T(8,128)(2,1)S(1)}, u32[]{:S(2)}, u32[]{:S(2)}) async-start(bf16[8,32,512]{2,1,0:T(8,128)(2,1)} %pad_maximum_fusion), calls=%async_computation.2 | async-start | bytes 524288 | tf_op jit(solution)/shard_map/all_to_all | solution.py:40
  35.0 7.4 %all-to-all-done.2 = bf16[8,32,512]{2,1,0:T(8,128)(2,1)S(1)} async-done(((bf16[8,32,512]{2,1,0:T(8,128)(2,1)}), bf16[8,32,512]{2,1,0:T(8,128)(2,1)S(1)}, u32[]{:S(2)}, u32[]{:S(2)}) %all-to-all-start.2) | async-done | bytes 262176 | tf_op jit(solution)/shard_map/all_to_all | solution.py:40
  44.3 8.5 %all_to_all.52 = bf16[8,32,256]{2,1,0:T(8,128)(2,1)S(1)} all-to-all(bf16[8,32,256]{2,1,0:T(8,128)(2,1)S(1)} %broadcast_in_dim.30), channel_id=1, replica_groups=mesh['tp'=16,'dp'=8] {'dp'}, dimensions={0} | all-to-all | bytes 262144 | tf_op jit(solution)/shard_map/all_to_all | solution.py:15
  53.0 11.6 %all_to_all.53 = bf16[16,16,512]{2,1,0:T(8,128)(2,1)S(1)} all-to-all(bf16[16,16,512]{2,1,0:T(8,128)(2,1)S(1)} %bitcast.126), channel_id=1, replica_groups=mesh['tp'=16,'dp'=8] {'tp'}, dimensions={0} | all-to-all | bytes 524288 | tf_op jit(solution)/shard_map/all_to_all | solution.py:40
  65.4 7.6 %all_to_all.54 = f32[8,1,16]{2,1,0:T(1,128)S(1)} all-to-all(f32[8,1,16]{2,1,0:T(1,128)S(1)} %broadcast_in_dim.31), channel_id=1, replica_groups=mesh['tp'=16,'dp'=8] {'dp'}, dimensions={0} | all-to-all | bytes 1024 | tf_op jit(solution)/shard_map/all_to_all | solution.py:15
  73.2 0.7 broadcast_in_dim.32
  73.9 3.5 %all-to-all-start.6 = ((bf16[16,16,512]{2,1,0:T(8,128)(2,1)}), bf16[16,16,512]{2,1,0:T(8,128)(2,1)S(1)}, u32[]{:S(2)}, u32[]{:S(2)}) async-start(bf16[16,16,512]{2,1,0:T(8,128)(2,1)} %broadcast_in_dim.32), calls=%async_computation.6 | async-start | bytes 524288 | tf_op jit(solution)/shard_map/all_to_all | solution.py:15
  77.5 8.9 %all-to-all-done.6 = bf16[16,16,512]{2,1,0:T(8,128)(2,1)S(1)} async-done(((bf16[16,16,512]{2,1,0:T(8,128)(2,1)}), bf16[16,16,512]{2,1,0:T(8,128)(2,1)S(1)}, u32[]{:S(2)}, u32[]{:S(2)}) %all-to-all-start.6) | async-done | bytes 262176 | tf_op jit(solution)/shard_map/all_to_all | solution.py:15
  86.8 0.7 pad_maximum_fusion.1
  87.6 3.4 %all-to-all-start.7 = ((bf16[8,32,512]{2,1,0:T(8,128)(2,1)}), bf16[8,32,512]{2,1,0:T(8,128)(2,1)S(1)}, u32[]{:S(2)}, u32[]{:S(2)}) async-start(bf16[8,32,512]{2,1,0:T(8,128)(2,1)} %pad_maximum_fusion.1), calls=%async_computation.7 | async-start | bytes 524288 | tf_op jit(solution)/shard_map/all_to_all | solution.py:40
  91.0 7.4 %all-to-all-done.7 = bf16[8,32,512]{2,1,0:T(8,128)(2,1)S(1)} async-done(((bf16[8,32,512]{2,1,0:T(8,128)(2,1)}), bf16[8,32,512]{2,1,0:T(8,128)(2,1)S(1)}, u32[]{:S(2)}, u32[]{:S(2)}) %all-to-all-start.7) | async-done | bytes 262176 | tf_op jit(solution)/shard_map/all_to_all | solution.py:40
  100.1 3.4 %all-to-all-start.8 = ((bf16[8,32,256]{2,1,0:T(8,128)(2,1)}), bf16[8,32,256]{2,1,0:T(8,128)(2,1)S(1)}, u32[]{:S(2)}, u32[]{:S(2)}) async-start(bf16[8,32,256]{2,1,0:T(8,128)(2,1)} %broadcast_in_dim.33), calls=%async_computation.8 | async-start | bytes 262144 | tf_op jit(solution)/shard_map/all_to_all | solution.py:15
  103.5 6.0 %all-to-all-done.8 = bf16[8,32,256]{2,1,0:T(8,128)(2,1)S(1)} async-done(((bf16[8,32,256]{2,1,0:T(8,128)(2,1)}), bf16[8,32,256]{2,1,0:T(8,128)(2,1)S(1)}, u32[]{:S(2)}, u32[]{:S(2)}) %all-to-all-start.8) | async-done | bytes 131104 | tf_op jit(solution)/shard_map/all_to_all | solution.py:15
  109.5 0.9 convolution_convert_fusion
  110.5 3.5 %all-to-all-start.9 = ((bf16[16,16,512]{2,1,0:T(8,128)(2,1)}), bf16[16,16,512]{2,1,0:T(8,128)(2,1)S(1)}, u32[]{:S(2)}, u32[]{:S(2)}) async-start(bf16[16,16,512]{2,1,0:T(8,128)(2,1)} %bitcast.47), calls=%async_computation.9 | async-start | bytes 524288 | tf_op jit(solution)/shard_map/all_to_all | solution.py:40
  115.3 7.4 %all-to-all-done.9 = bf16[16,16,512]{2,1,0:T(8,128)(2,1)S(1)} async-done(((bf16[16,16,512]{2,1,0:T(8,128)(2,1)}), bf16[16,16,512]{2,1,0:T(8,128)(2,1)S(1)}, u32[]{:S(2)}, u32[]{:S(2)}) %all-to-all-start.9) | async-done | bytes 262176 | tf_op jit(solution)/shard_map/all_to_all | solution.py:40
  (70 shorter events, 9.0 us)
Async XLA Ops:
  0.6 29.6 %copy-start = (bf16[2,512,256]{2,1,0:T(8,128)(2,1)S(1)}, bf16[2,512,256]{2,1,0:T(8,128)(2,1)}, u32[]{:S(2)}) copy-start(bf16[2,512,256]{2,1,0:T(8,128)(2,1)} %param.16) | copy-start | bytes 1572868
  2.1 9.8 %all-to-all-start = ((f32[8,1,16]{2,1,0:T(1,128)}), f32[8,1,16]{2,1,0:T(1,128)S(1)}, u32[]{:S(2)}, u32[]{:S(2)}) async-start(f32[8,1,16]{2,1,0:T(1,128)} %broadcast_in_dim.28), calls=%async_computation | async-start | bytes 8192 | tf_op jit(solution)/shard_map/all_to_all | solution.py:15
  12.8 8.7 %copy-start.6 = (f32[2,4,256]{2,1,0:T(4,128)S(1)}, f32[2,4,256]{2,1,0:T(4,128)}, u32[]{:S(2)}) copy-start(f32[2,4,256]{2,1,0:T(4,128)} %param.17) | copy-start | bytes 24580
  13.5 16.9 %copy-start.1 = (bf16[2,512,256]{2,1,0:T(8,128)(2,1)S(1)}, bf16[2,512,256]{2,1,0:T(8,128)(2,1)}, u32[]{:S(2)}) copy-start(bf16[2,512,256]{2,1,0:T(8,128)(2,1)} %param.15) | copy-start | bytes 1572868
  13.5 16.7 %all-to-all-start.1 = ((bf16[16,16,512]{2,1,0:T(8,128)(2,1)}), bf16[16,16,512]{2,1,0:T(8,128)(2,1)S(1)}, u32[]{:S(2)}, u32[]{:S(2)}) async-start(bf16[16,16,512]{2,1,0:T(8,128)(2,1)} %broadcast_in_dim.29), calls=%async_computation.1 | async-start | bytes 524288 | tf_op jit(solution)/shard_map/all_to_all | solution.py:15
  31.4 3.6 %copy-start.7 = (f32[2,256]{1,0:T(2,128)S(1)}, f32[2,256]{1,0:T(2,128)}, u32[]{:S(2)}) copy-start(f32[2,256]{1,0:T(2,128)} %param.20) | copy-start | bytes 6148
  31.4 3.6 %copy-start.4 = (bf16[2,32,3,256]{3,1,2,0:T(8,128)(2,1)S(1)}, bf16[2,32,3,256]{3,1,2,0:T(8,128)(2,1)}, u32[]{:S(2)}) copy-start(bf16[2,32,3,256]{3,1,2,0:T(8,128)(2,1)} %param.13) | copy-start | bytes 294916
  31.4 11.0 %all-to-all-start.2 = ((bf16[8,32,512]{2,1,0:T(8,128)(2,1)}), bf16[8,32,512]{2,1,0:T(8,128)(2,1)S(1)}, u32[]{:S(2)}, u32[]{:S(2)}) async-start(bf16[8,32,512]{2,1,0:T(8,128)(2,1)} %pad_maximum_fusion), calls=%async_computation.2 | async-start | bytes 524288 | tf_op jit(solution)/shard_map/all_to_all | solution.py:40
  35.0 7.5 %copy-start.8 = (f32[2,4,64,64]{3,2,1,0:T(8,128)S(1)}, f32[2,4,64,64]{3,2,1,0:T(8,128)}, u32[]{:S(2)}) copy-start(f32[2,4,64,64]{3,2,1,0:T(8,128)} %param.19) | copy-start | bytes 393220
  42.4 1.0 copy-start.9
  43.4 0.8 copy-start.5
  43.6 9.1 %copy-start.2 = (bf16[2,256,512]{2,1,0:T(8,128)(2,1)S(1)}, bf16[2,256,512]{2,1,0:T(8,128)(2,1)}, u32[]{:S(2)}) copy-start(bf16[2,256,512]{2,1,0:T(8,128)(2,1)} %param.21) | copy-start | bytes 1572868
  64.6 0.7 copy-start.3
  73.9 12.4 %all-to-all-start.6 = ((bf16[16,16,512]{2,1,0:T(8,128)(2,1)}), bf16[16,16,512]{2,1,0:T(8,128)(2,1)S(1)}, u32[]{:S(2)}, u32[]{:S(2)}) async-start(bf16[16,16,512]{2,1,0:T(8,128)(2,1)} %broadcast_in_dim.32), calls=%async_computation.6 | async-start | bytes 524288 | tf_op jit(solution)/shard_map/all_to_all | solution.py:15
  87.6 10.8 %all-to-all-start.7 = ((bf16[8,32,512]{2,1,0:T(8,128)(2,1)}), bf16[8,32,512]{2,1,0:T(8,128)(2,1)S(1)}, u32[]{:S(2)}, u32[]{:S(2)}) async-start(bf16[8,32,512]{2,1,0:T(8,128)(2,1)} %pad_maximum_fusion.1), calls=%async_computation.7 | async-start | bytes 524288 | tf_op jit(solution)/shard_map/all_to_all | solution.py:40
  100.1 9.4 %all-to-all-start.8 = ((bf16[8,32,256]{2,1,0:T(8,128)(2,1)}), bf16[8,32,256]{2,1,0:T(8,128)(2,1)S(1)}, u32[]{:S(2)}, u32[]{:S(2)}) async-start(bf16[8,32,256]{2,1,0:T(8,128)(2,1)} %broadcast_in_dim.33), calls=%async_computation.8 | async-start | bytes 262144 | tf_op jit(solution)/shard_map/all_to_all | solution.py:15
  110.5 12.3 %all-to-all-start.9 = ((bf16[16,16,512]{2,1,0:T(8,128)(2,1)}), bf16[16,16,512]{2,1,0:T(8,128)(2,1)S(1)}, u32[]{:S(2)}, u32[]{:S(2)}) async-start(bf16[16,16,512]{2,1,0:T(8,128)(2,1)} %bitcast.47), calls=%async_computation.9 | async-start | bytes 524288 | tf_op jit(solution)/shard_map/all_to_all | solution.py:40
where the time goes:
time: 125 us; the launch traced here: 123 us
  waiting for transfers between devices  50.2 us (40%)
  starting transfers between devices  30 us (24%)
  blocking collectives  27.7 us (22%)
  local copies, waits for them, and re-layouts  5.85 us (5%)
  other arithmetic  5.62 us (4%)
  matrix products  3.05 us (2%)
    all_to_all x4, waiting for transfers between devices, from_everyone(): return lax.all_to_all(copies, axis, split_axis=0, concat_axis=0, tiled=True)  28 us
    all_to_all x3, waiting for transfers between devices, sum_at_owner(): lax.all_to_all(parts, axis, split_axis=0, concat_axis=0, tiled=True)  22.2 us
    all_to_all x4, starting transfers between devices, from_everyone(): return lax.all_to_all(copies, axis, split_axis=0, concat_axis=0, tiled=True)  19.5 us
    all_to_all x2, blocking collectives, from_everyone(): return lax.all_to_all(copies, axis, split_axis=0, concat_axis=0, tiled=True)  16.1 us
    all_to_all x1, blocking collectives, sum_at_owner(): lax.all_to_all(parts, axis, split_axis=0, concat_axis=0, tiled=True)  11.6 us
    all_to_all x3, starting transfers between devices, sum_at_owner(): lax.all_to_all(parts, axis, split_axis=0, concat_axis=0, tiled=True)  10.5 us
    broadcast_in_dim x6, local copies, waits for them, and re-layouts, from_everyone(): copies = jnp.broadcast_to(array, (lax.axis_size(axis), *array.shape))  2.74 us
  transfers between devices with their start and end apart: 7, of which 7 were waited for; matrix products, arithmetic and copies ran while one was open for 2% of the time, Pallas kernels for 0%

commit v1 on v0

--- a/solution.py
+++ b/solution.py
@@ -41,32 +41,31 @@
     return arrived.astype(jnp.float32).sum(axis=0)
 
 
-def scaled(rows, gain):
-    rowsf = rows.astype(jnp.float32)
-    sumsq = of_everyone(jnp.sum(rowsf * rowsf, axis=1), "dp")
-    return (rowsf * lax.rsqrt(sumsq / D + EPS)[:, None] * gain[None, :]).astype(jnp.bfloat16)
-
-
-def shard_inputs(normed, path_w, gate_branch_matrix):
+def split_inputs(rows, gain, path_w, gate_branch_matrix):
+    everyone = collect(rows, "tp", 0).astype(jnp.float32)
+    sumsq = jnp.sum(everyone * everyone, axis=1, keepdims=True)
+    high = lax.reduce_precision(sumsq, 8, 7)
+    low = sumsq - high
+    gained = (everyone * gain[None, :]).astype(jnp.bfloat16)
     return jnp.concatenate(
         [
-            jnp.dot(normed, path_w, preferred_element_type=jnp.float32),
-            jnp.dot(normed, gate_branch_matrix, preferred_element_type=jnp.float32),
+            jnp.dot(gained, path_w, preferred_element_type=jnp.float32),
+            jnp.dot(gained, gate_branch_matrix, preferred_element_type=jnp.float32),
+            high,
+            low,
+            jnp.zeros((sumsq.shape[0], 126), jnp.float32),
         ],
         axis=1,
     )
 
 
-def split_inputs(rows, gain, path_w, gate_branch_matrix):
-    normed = scaled(rows, gain)
-    return shard_inputs(collect(normed, "tp", 0), path_w, gate_branch_matrix)
-
-
 def recur_tail(partial_value, hidden, buffer, taps, recur_w, input_matrix, logit, out_w):
-    width = partial_value.shape[1] // 2
+    width = (partial_value.shape[1] - 128) // 2
     summed = sum_at_owner(partial_value.astype(jnp.bfloat16), "dp", 0)
-    zpath = summed[:, :width].astype(jnp.bfloat16)
-    zgate = summed[:, width:].astype(jnp.bfloat16)
+    sumsq = summed[:, 2 * width] + summed[:, 2 * width + 1]
+    factor = lax.rsqrt(sumsq / D + EPS)[:, None]
+    zpath = (summed[:, :width] * factor).astype(jnp.bfloat16)
+    zgate = (summed[:, width : 2 * width] * factor).astype(jnp.bfloat16)
     batch = zpath.shape[0]
     conv = zpath.astype(jnp.float32) * taps[TAPS - 1][None, :]
     for j in range(TAPS - 1):

time: 125 us -> 107 us (0.86)
  waiting for transfers between devices: 50.2 us -> 29.5 us
  blocking collectives: 27.7 us -> 42.3 us
  starting transfers between devices: 30 us -> 19.6 us
  other arithmetic: 5.62 us -> 3.15 us
  local copies, waits for them, and re-layouts: 5.85 us -> 7.68 us
    all_to_all x4 -> x2, waiting for transfers between devices: 28 us -> 14 us  [from_everyone(): return lax.all_to_all(copies, axis, split_axis=0, concat_axis=0, tiled=True)]
    all_to_all x1 -> x2, blocking collectives: 11.6 us -> 22.2 us  [sum_at_owner(): lax.all_to_all(parts, axis, split_axis=0, concat_axis=0, tiled=True)]
    all_to_all x4 -> x2, starting transfers between devices: 19.5 us -> 11.5 us  [from_everyone(): return lax.all_to_all(copies, axis, split_axis=0, concat_axis=0, tiled=True)]
    all_to_all x3 -> x2, waiting for transfers between devices: 22.2 us -> 15.6 us  [sum_at_owner(): lax.all_to_all(parts, axis, split_axis=0, concat_axis=0, tiled=True)]
    all_to_all x2, blocking collectives: 16.1 us -> 20.1 us  [from_everyone(): return lax.all_to_all(copies, axis, split_axis=0, concat_axis=0, tiled=True)]
    all_to_all x3 -> x2, starting transfers between devices: 10.5 us -> 8.13 us  [sum_at_owner(): lax.all_to_all(parts, axis, split_axis=0, concat_axis=0, tiled=True)]
    unnamed x20 -> x22, local copies, waits for them, and re-layouts: 1.52 us -> 2.98 us
    concatenate x2 -> x0, other arithmetic: 1.44 us -> none  [shard_inputs(): jnp.concatenate([jnp.dot(normed, path_w, preferred_element_type=jnp.float...]
  transfers between devices with their start and end apart: 7 -> 4, of which waited for: 7 -> 4; matrix products, arithmetic and copies ran while one was open for 2% -> 1% of each run, Pallas kernels for 0% -> 0%
where the time goes in v1:
time: 107 us; the launch traced here: 106 us
  blocking collectives  42.3 us (40%)
  waiting for transfers between devices  29.5 us (28%)
  starting transfers between devices  19.6 us (18%)
  local copies, waits for them, and re-layouts  7.68 us (7%)
  other arithmetic  3.15 us (3%)
  matrix products  3.07 us (3%)
    all_to_all x2, blocking collectives, sum_at_owner(): lax.all_to_all(parts, axis, split_axis=0, concat_axis=0, tiled=True)  22.2 us
    all_to_all x2, blocking collectives, from_everyone(): return lax.all_to_all(copies, axis, split_axis=0, concat_axis=0, tiled=True)  20.1 us
    all_to_all x2, waiting for transfers between devices, sum_at_owner(): lax.all_to_all(parts, axis, split_axis=0, concat_axis=0, tiled=True)  15.6 us
    all_to_all x2, waiting for transfers between devices, from_everyone(): return lax.all_to_all(copies, axis, split_axis=0, concat_axis=0, tiled=True)  14 us
    all_to_all x2, starting transfers between devices, from_everyone(): return lax.all_to_all(copies, axis, split_axis=0, concat_axis=0, tiled=True)  11.5 us
    all_to_all x2, starting transfers between devices, sum_at_owner(): lax.all_to_all(parts, axis, split_axis=0, concat_axis=0, tiled=True)  8.13 us
    unnamed x22, local copies, waits for them, and re-layouts  2.98 us
  transfers between devices with their start and end apart: 4, of which 4 were waited for; matrix products, arithmetic and copies ran while one was open for 1% of the time, Pallas kernels for 0%

profile of v1, /device:TPU:0, one launch (start us, length us, event | category | flops | bytes accessed | tf_op | source)
XLA Modules:
  0.0 106.2 jit_solution(17394979601101228045)
XLA Ops:
  0.6 1.4 %broadcast_in_dim.24 = bf16[16,16,512]{2,1,0:T(8,128)(2,1)} broadcast(bf16[16,512]{1,0:T(8,128)(2,1)} %param.11), dimensions={1,2} | broadcast | bytes 278528 | tf_op jit(solution)/shard_map/broadcast_in_dim | solution.py:14
  2.1 8.1 %all-to-all-start = ((bf16[16,16,512]{2,1,0:T(8,128)(2,1)}), bf16[16,16,512]{2,1,0:T(8,128)(2,1)S(1)}, u32[]{:S(2)}, u32[]{:S(2)}) async-start(bf16[16,16,512]{2,1,0:T(8,128)(2,1)} %broadcast_in_dim.24), calls=%async_computation | async-start | bytes 524288 | tf_op jit(solution)/shard_map/all_to_all | solution.py:15
  10.3 0.7 copy-done.6
  10.9 8.0 %all-to-all-done = bf16[16,16,512]{2,1,0:T(8,128)(2,1)S(1)} async-done(((bf16[16,16,512]{2,1,0:T(8,128)(2,1)}), bf16[16,16,512]{2,1,0:T(8,128)(2,1)S(1)}, u32[]{:S(2)}, u32[]{:S(2)}) %all-to-all-start) | async-done | bytes 262176 | tf_op jit(solution)/shard_map/all_to_all | solution.py:15
  19.3 0.6 copy-done.1
  20.6 0.9 concatenate.19
  21.4 4.6 %all-to-all-start.1 = ((bf16[8,32,640]{2,1,0:T(8,128)(2,1)}), bf16[8,32,640]{2,1,0:T(8,128)(2,1)S(1)}, u32[]{:S(2)}, u32[]{:S(2)}) async-start(bf16[8,32,640]{2,1,0:T(8,128)(2,1)} %concatenate.19), calls=%async_computation.1 | async-start | bytes 655360 | tf_op jit(solution)/shard_map/all_to_all | solution.py:40
  26.1 8.1 %all-to-all-done.1 = bf16[8,32,640]{2,1,0:T(8,128)(2,1)S(1)} async-done(((bf16[8,32,640]{2,1,0:T(8,128)(2,1)}), bf16[8,32,640]{2,1,0:T(8,128)(2,1)S(1)}, u32[]{:S(2)}, u32[]{:S(2)}) %all-to-all-start.1) | async-done | bytes 327712 | tf_op jit(solution)/shard_map/all_to_all | solution.py:40
  35.1 0.5 copy-done.10
  36.1 0.4 copy-done.5
  36.6 8.5 %all_to_all.40 = bf16[8,32,256]{2,1,0:T(8,128)(2,1)S(1)} all-to-all(bf16[8,32,256]{2,1,0:T(8,128)(2,1)S(1)} %broadcast_in_dim.25), channel_id=1, replica_groups=mesh['tp'=16,'dp'=8] {'dp'}, dimensions={0} | all-to-all | bytes 262144 | tf_op jit(solution)/shard_map/all_to_all | solution.py:15
  45.3 11.6 %all_to_all.41 = bf16[16,16,512]{2,1,0:T(8,128)(2,1)S(1)} all-to-all(bf16[16,16,512]{2,1,0:T(8,128)(2,1)S(1)} %bitcast.124), channel_id=1, replica_groups=mesh['tp'=16,'dp'=8] {'tp'}, dimensions={0} | all-to-all | bytes 524288 | tf_op jit(solution)/shard_map/all_to_all | solution.py:40
  57.0 0.7 copy-done.4
  57.7 11.6 %all_to_all.42 = bf16[16,16,512]{2,1,0:T(8,128)(2,1)S(1)} all-to-all(bf16[16,16,512]{2,1,0:T(8,128)(2,1)S(1)} %broadcast_in_dim.26), channel_id=1, replica_groups=mesh['tp'=16,'dp'=8] {'tp'}, dimensions={0} | all-to-all | bytes 524288 | tf_op jit(solution)/shard_map/all_to_all | solution.py:15
  70.4 10.6 %all_to_all.43 = bf16[8,32,640]{2,1,0:T(8,128)(2,1)S(1)} all-to-all(bf16[8,32,640]{2,1,0:T(8,128)(2,1)S(1)} %concatenate.20), channel_id=1, replica_groups=mesh['tp'=16,'dp'=8] {'dp'}, dimensions={0} | all-to-all | bytes 655360 | tf_op jit(solution)/shard_map/all_to_all | solution.py:40
  82.3 0.7 broadcast_in_dim.27
  83.0 3.4 %all-to-all-start.6 = ((bf16[8,32,256]{2,1,0:T(8,128)(2,1)}), bf16[8,32,256]{2,1,0:T(8,128)(2,1)S(1)}, u32[]{:S(2)}, u32[]{:S(2)}) async-start(bf16[8,32,256]{2,1,0:T(8,128)(2,1)} %broadcast_in_dim.27), calls=%async_computation.6 | async-start | bytes 262144 | tf_op jit(solution)/shard_map/all_to_all | solution.py:15
  86.4 6.0 %all-to-all-done.6 = bf16[8,32,256]{2,1,0:T(8,128)(2,1)S(1)} async-done(((bf16[8,32,256]{2,1,0:T(8,128)(2,1)}), bf16[8,32,256]{2,1,0:T(8,128)(2,1)S(1)}, u32[]{:S(2)}, u32[]{:S(2)}) %all-to-all-start.6) | async-done | bytes 131104 | tf_op jit(solution)/shard_map/all_to_all | solution.py:15
  92.4 0.9 convolution_convert_fusion
  93.3 3.5 %all-to-all-start.7 = ((bf16[16,16,512]{2,1,0:T(8,128)(2,1)}), bf16[16,16,512]{2,1,0:T(8,128)(2,1)S(1)}, u32[]{:S(2)}, u32[]{:S(2)}) async-start(bf16[16,16,512]{2,1,0:T(8,128)(2,1)} %bitcast.45), calls=%async_computation.7 | async-start | bytes 524288 | tf_op jit(solution)/shard_map/all_to_all | solution.py:40
  96.9 0.6 pad_maximum_fusion.1
  97.5 0.7 pad_maximum_fusion
  98.2 7.4 %all-to-all-done.7 = bf16[16,16,512]{2,1,0:T(8,128)(2,1)S(1)} async-done(((bf16[16,16,512]{2,1,0:T(8,128)(2,1)}), bf16[16,16,512]{2,1,0:T(8,128)(2,1)S(1)}, u32[]{:S(2)}, u32[]{:S(2)}) %all-to-all-start.7) | async-done | bytes 262176 | tf_op jit(solution)/shard_map/all_to_all | solution.py:40
  105.6 0.6 add_convert_fusion
  (69 shorter events, 5.2 us)
Async XLA Ops:
  0.6 9.6 %copy-start.7 = (f32[2,512]{1,0:T(2,128)S(1)}, f32[2,512]{1,0:T(2,128)}, u32[]{:S(2)}) copy-start(f32[2,512]{1,0:T(2,128)} %param.14) | copy-start | bytes 12292
  2.1 17.0 %copy-start = (bf16[2,512,256]{2,1,0:T(8,128)(2,1)S(1)}, bf16[2,512,256]{2,1,0:T(8,128)(2,1)}, u32[]{:S(2)}) copy-start(bf16[2,512,256]{2,1,0:T(8,128)(2,1)} %param.16) | copy-start | bytes 1572868
  2.1 16.8 %all-to-all-start = ((bf16[16,16,512]{2,1,0:T(8,128)(2,1)}), bf16[16,16,512]{2,1,0:T(8,128)(2,1)S(1)}, u32[]{:S(2)}, u32[]{:S(2)}) async-start(bf16[16,16,512]{2,1,0:T(8,128)(2,1)} %broadcast_in_dim.24), calls=%async_computation | async-start | bytes 524288 | tf_op jit(solution)/shard_map/all_to_all | solution.py:15
  10.2 0.7 copy-start.6
  18.9 1.0 copy-start.1
  21.4 4.6 %copy-start.8 = (f32[2,256]{1,0:T(2,128)S(1)}, f32[2,256]{1,0:T(2,128)}, u32[]{:S(2)}) copy-start(f32[2,256]{1,0:T(2,128)} %param.20) | copy-start | bytes 6148
  21.4 4.6 %copy-start.3 = (bf16[2,32,3,256]{3,1,2,0:T(8,128)(2,1)S(1)}, bf16[2,32,3,256]{3,1,2,0:T(8,128)(2,1)}, u32[]{:S(2)}) copy-start(bf16[2,32,3,256]{3,1,2,0:T(8,128)(2,1)} %param.13) | copy-start | bytes 294916
  21.4 12.8 %all-to-all-start.1 = ((bf16[8,32,640]{2,1,0:T(8,128)(2,1)}), bf16[8,32,640]{2,1,0:T(8,128)(2,1)S(1)}, u32[]{:S(2)}, u32[]{:S(2)}) async-start(bf16[8,32,640]{2,1,0:T(8,128)(2,1)} %concatenate.19), calls=%async_computation.1 | async-start | bytes 655360 | tf_op jit(solution)/shard_map/all_to_all | solution.py:40
  26.1 8.6 %copy-start.9 = (f32[2,4,64,64]{3,2,1,0:T(8,128)S(1)}, f32[2,4,64,64]{3,2,1,0:T(8,128)}, u32[]{:S(2)}) copy-start(f32[2,4,64,64]{3,2,1,0:T(8,128)} %param.18) | copy-start | bytes 393220
  34.7 1.0 copy-start.10
  35.6 0.8 copy-start.5
  35.9 9.2 %copy-start.2 = (bf16[2,256,512]{2,1,0:T(8,128)(2,1)S(1)}, bf16[2,256,512]{2,1,0:T(8,128)(2,1)}, u32[]{:S(2)}) copy-start(bf16[2,256,512]{2,1,0:T(8,128)(2,1)} %param.21) | copy-start | bytes 1572868
  56.9 0.7 copy-start.4
  83.0 9.4 %all-to-all-start.6 = ((bf16[8,32,256]{2,1,0:T(8,128)(2,1)}), bf16[8,32,256]{2,1,0:T(8,128)(2,1)S(1)}, u32[]{:S(2)}, u32[]{:S(2)}) async-start(bf16[8,32,256]{2,1,0:T(8,128)(2,1)} %broadcast_in_dim.27), calls=%async_computation.6 | async-start | bytes 262144 | tf_op jit(solution)/shard_map/all_to_all | solution.py:15
  93.3 12.3 %all-to-all-start.7 = ((bf16[16,16,512]{2,1,0:T(8,128)(2,1)}), bf16[16,16,512]{2,1,0:T(8,128)(2,1)S(1)}, u32[]{:S(2)}, u32[]{:S(2)}) async-start(bf16[16,16,512]{2,1,0:T(8,128)(2,1)} %bitcast.45), calls=%async_computation.7 | async-start | bytes 524288 | tf_op jit(solution)/shard_map/all_to_all | solution.py:40
